TPU v7x, 32 devices: a whole 2x2x4 slice. The times are simulated.
32 devices in a mesh: sp: 8 (over z, x), tp: 4 (over y, core).
Axes of the slice: x: 2, y: 2, z: 4, core: 2. Of those that a mesh axis runs over, the one named last changes fastest.
Arguments:
- residual: bfloat16 [4096, 2048], P('sp'), may hold values from -6 to 6
- queries: bfloat16 [4096, 1024], P('sp', 'tp'), may hold values from -384 to 384
- key_pairs: bfloat16 [4096, 1024], P('sp', 'tp'), may hold values from -384 to 384
- values: bfloat16 [4096, 1024], P('sp', 'tp'), may hold values from -6 to 6
- lambdas: float32 [8], P('tp'), may hold values from 0.3 to 0.8
- head_gain: float32 [128], replicated, may hold values from 0.1 to 1.9
- w_out: bfloat16 [1024, 2048], replicated, may hold values from -0.1875 to 0.1875
- norm_gain: float32 [2048], replicated, may hold values from 0.1 to 1.9
- w_gate: bfloat16 [2048, 5632], P('sp', 'tp'), may hold values from -0.125 to 0.125
- w_up: bfloat16 [2048, 5632], P('sp', 'tp'), may hold values from -0.125 to 0.125
- w_down: bfloat16 [5632, 2048], P('tp', 'sp'), may hold values from -0.078125 to 0.078125
Outputs:
- layer_out: bfloat16 [4096, 2048], P(('sp', 'tp'))
All inputs are finite; a program needn't handle non-finite values.
Results may differ from a plain program's by a relative error of at most 0.018.
Values may be sent and summed in bfloat16 or wider, within the bound.
A program may use at most 128 MiB of HBM per device.

v0:
```python
import math
import jax
import jax.numpy as jnp
from jax import lax
from jax.sharding import PartitionSpec as P

HD = 64


def per_device(
    residual, queries, key_pairs, values, lambdas, head_gain, w_out, norm_gain, w_gate, w_up, w_down
):
    local_rows = queries.shape[0]
    heads_here = lambdas.shape[0]
    value_width = values.shape[1] // heads_here
    score_scale = HD ** (-0.5)
    query_view = queries.reshape(local_rows, heads_here, 2, HD)

    def update(carry, key_block, value_block):
        highest, totals, mixture = carry
        scores = (
            jnp.einsum("qhmd,khmd->hmqk", query_view, key_block, preferred_element_type=jnp.float32)
            * score_scale
        )
        new_high = jnp.maximum(highest, jnp.max(scores, axis=-1))
        shrink = jnp.exp(highest - new_high)
        weights = jnp.exp(scores - new_high[..., None])
        totals = totals * shrink + jnp.sum(weights, axis=-1)
        mixture = mixture * shrink[..., None] + jnp.einsum(
            "hmqk,khe->hmqe",
            weights.astype(jnp.bfloat16),
            value_block,
            preferred_element_type=jnp.float32,
        )
        return (new_high, totals, mixture)

    initial = (
        jnp.full((heads_here, 2, local_rows), -jnp.inf, jnp.float32),
        jnp.zeros((heads_here, 2, local_rows), jnp.float32),
        jnp.zeros((heads_here, 2, local_rows, value_width), jnp.float32),
    )
    key_piece = lax.all_gather(key_pairs, "sp", axis=0, tiled=True)
    value_piece = lax.all_gather(values, "sp", axis=0, tiled=True)
    length = key_piece.shape[0]
    span = math.gcd(length, 512)
    key_blocks = key_piece.reshape(length // span, span, heads_here, 2, HD)
    value_blocks = value_piece.reshape(length // span, span, heads_here, value_width)

    def advance(position, inner):
        return update(inner, key_blocks[position], value_blocks[position])

    highest, totals, mixture = lax.fori_loop(0, length // span, advance, initial)
    mixed = mixture / totals[..., None]
    differ = mixed[:, 0] - lambdas[:, None, None] * mixed[:, 1]
    normed_heads = (
        differ * lax.rsqrt(jnp.mean(differ * differ, axis=-1, keepdims=True) + 1e-05) * head_gain
    )
    heads_out = (
        jnp.transpose(normed_heads, (1, 0, 2))
        .reshape(local_rows, heads_here * value_width)
        .astype(jnp.bfloat16)
    )
    tp_index = lax.axis_index("tp")
    own_rows = local_rows // lax.axis_size("tp")
    own_begin = tp_index * own_rows
    w_mine = lax.dynamic_slice_in_dim(
        w_out, tp_index * heads_here * value_width, heads_here * value_width, 0
    )
    projected = lax.psum_scatter(
        jnp.dot(heads_out, w_mine, preferred_element_type=jnp.float32).astype(jnp.bfloat16),
        "tp",
        scatter_dimension=0,
        tiled=True,
    ).astype(jnp.float32)
    residual_own = lax.dynamic_slice_in_dim(residual, own_begin, own_rows, 0)
    hidden_own = (residual_own.astype(jnp.float32) + projected).astype(jnp.bfloat16)
    stream_f = hidden_own.astype(jnp.float32)
    scaled = stream_f * lax.rsqrt(jnp.mean(stream_f * stream_f, axis=-1, keepdims=True) + 1e-05)
    normed_rows = lax.all_gather(
        (scaled * norm_gain).astype(jnp.bfloat16), "tp", axis=0, tiled=True
    )
    unit_width = w_gate.shape[1]
    joined = jnp.concatenate([w_gate, w_up], axis=1)
    both_sums = jnp.dot(
        normed_rows,
        lax.all_gather(joined, "sp", axis=0, tiled=True),
        preferred_element_type=jnp.float32,
    )
    gate_sum = both_sums[:, :unit_width]
    up_sum = both_sums[:, unit_width:]
    hidden_units = (jax.nn.silu(gate_sum) * up_sum).astype(jnp.bfloat16)
    down_whole = lax.all_gather(w_down, "sp", axis=1, tiled=True)
    ffn_out = lax.psum_scatter(
        jnp.dot(hidden_units, down_whole, preferred_element_type=jnp.float32).astype(jnp.bfloat16),
        "tp",
        scatter_dimension=0,
        tiled=True,
    ).astype(jnp.float32)
    return (hidden_own.astype(jnp.float32) + ffn_out).astype(jnp.bfloat16)


def solution(mesh):
    placed = (
        P("sp", None),
        P("sp", "tp"),
        P("sp", "tp"),
        P("sp", "tp"),
        P("tp"),
        P(),
        P(),
        P(),
        P("sp", "tp"),
        P("sp", "tp"),
        P("tp", "sp"),
    )
    return jax.shard_map(
        per_device, mesh=mesh, in_specs=placed, out_specs=P(("sp", "tp"), None), check_vma=False
    )
```

profile of v0, /device:TPU:0, one launch (start us, length us, event | category | flops | bytes accessed | tf_op | source)
XLA Modules:
  0.0 547.7 jit_solution(14696506700024109413)
XLA Ops:
  6.5 0.7 all-gather.6.cloned.1.call-update
  7.3 0.7 all-gather.8.cloned.1.call-update
  8.0 0.0 reduce-scatter.3.cloned.1.call-start
  8.1 1.1 copy.17
  9.2 52.1 %all-gather.6.cloned.1.call-done = bf16[4096,256]{1,0:T(8,128)(2,1)} async-done(((bf16[512,256]{1,0:T(8,128)(2,1)}), bf16[4096,256]{1,0:T(8,128)(2,1)}) %all-gather.6.cloned.1.call-update) | async-done | bytes 2097168 | tf_op jit(solution)/shard_map/all_gather | solution.py:42
  61.3 8.3 %reshape.37 = bf16[8,512,2,2,64]{4,3,2,1,0:T(2,128)(2,1)} reshape(bf16[4096,256]{1,0:T(8,128)(2,1)} %all-gather.6.cloned.1.call-done) | data formatting | bytes 4194304 | tf_op jit(solution)/shard_map/reshape | solution.py:46
  69.6 9.1 %copy.19 = bf16[8,512,2,2,64]{1,4,3,2,0:T(8,128)(2,1)S(1)} copy(bf16[8,512,2,2,64]{4,3,2,1,0:T(2,128)(2,1)} %reshape.37) | data formatting | bytes 4194304
  78.7 32.4 %all-gather.8.cloned.1.call-done = bf16[4096,256]{1,0:T(8,128)(2,1)} async-done(((bf16[512,256]{1,0:T(8,128)(2,1)}), bf16[4096,256]{1,0:T(8,128)(2,1)}) %all-gather.8.cloned.1.call-update) | async-done | bytes 2097168 | tf_op jit(solution)/shard_map/all_gather | solution.py:43
  111.1 4.0 reshape.38
  115.0 67.2 %while.18 = (s32[]{:T(128)}, f32[2,2,512]{2,1,0:T(2,128)S(1)}, f32[2,2,512]{2,1,0:T(2,128)S(1)}, f32[2,2,512,128]{3,2,1,0:T(8,128)S(1)}, bf16[8,512,2,2,64]{1,4,...) while((s32[]{:T(128)}, f32[2,2,512]{2,1,0:T(2,128)S(1)}, ...), condition=%wide.region_3.0_spmd.clone, body=%wide.region_0.0_spmd.clone.sunk | while | flops 411838464 | bytes 32899212 | solution.py:52
  115.0 2.7 bitcast_reduce_fusion.2
  117.7 3.0 fusion.44
  120.8 1.1 constant_dynamic-slice_fusion.2
  122.0 1.4 fusion.46
  123.4 2.7 bitcast_reduce_fusion.2
  126.1 3.0 fusion.44
  129.2 1.1 constant_dynamic-slice_fusion.2
  130.4 1.4 fusion.46
  131.8 2.7 bitcast_reduce_fusion.2
  134.5 3.0 fusion.44
  137.6 1.1 constant_dynamic-slice_fusion.2
  138.8 1.4 fusion.46
  140.2 2.7 bitcast_reduce_fusion.2
  142.9 3.0 fusion.44
  146.0 1.1 constant_dynamic-slice_fusion.2
  147.2 1.4 fusion.46
  148.6 2.7 bitcast_reduce_fusion.2
  151.3 3.0 fusion.44
  154.4 1.1 constant_dynamic-slice_fusion.2
  155.6 1.4 fusion.46
  157.0 2.7 bitcast_reduce_fusion.2
  159.7 3.0 fusion.44
  162.8 1.1 constant_dynamic-slice_fusion.2
  164.0 1.4 fusion.46
  165.4 2.7 bitcast_reduce_fusion.2
  168.1 3.0 fusion.44
  171.2 1.1 constant_dynamic-slice_fusion.2
  172.4 1.4 fusion.46
  173.8 2.7 bitcast_reduce_fusion.2
  176.5 3.0 fusion.44
  179.6 1.1 constant_dynamic-slice_fusion.2
  180.8 1.4 fusion.46
  182.2 0.3 copy.22
  182.6 0.2 broadcast_divide_fusion
  182.7 0.1 copy-done.4
  182.9 0.2 multiply_reduce_fusion
  183.1 0.1 multiply_convert_fusion
  183.2 3.3 convolution_convert_fusion
  186.6 0.0 all-gather.10.cloned.1.call-start
  186.6 29.8 %reduce-scatter.3.cloned.1.call-done = bf16[128,2048]{1,0:T(8,128)(2,1)} async-done(((bf16[512,2048]{1,0:T(8,128)(2,1)}), bf16[128,2048]{1,0:T(8,128)(2,1)}) %reduce-scatter.3.cloned.1.call-update) | async-done | bytes 524304 | tf_op jit(solution)/shard_map/reduce_scatter | solution.py:69
  216.4 1.5 fusion.20
  217.9 1.0 fusion.22
  218.9 0.0 all-gather.12.cloned.1.call-start
  219.0 1.2 pad_maximum_fusion
  220.2 0.0 all-gather.14.cloned.1.call-start
  220.3 0.5 all-gather.14.cloned.1.call-update
  220.8 0.2 reduce-scatter.5.cloned.1.call-start
  221.0 20.6 %all-gather.10.cloned.1.call-done = bf16[512,2048]{1,0:T(8,128)(2,1)} async-done(((bf16[128,2048]{1,0:T(8,128)(2,1)}), bf16[512,2048]{1,0:T(8,128)(2,1)}) %all-gather.10.cloned.1.call-update) | async-done | bytes 2097168 | tf_op jit(solution)/shard_map/all_gather | solution.py:79
  241.6 165.4 %all-gather.12.cloned.1.call-done = bf16[2048,2816]{1,0:T(8,128)(2,1)} async-done(((bf16[256,2816]{1,0:T(8,128)(2,1)}), bf16[2048,2816]{1,0:T(8,128)(2,1)}) %all-gather.12.cloned.1.call-update) | async-done | bytes 11534352 | tf_op jit(solution)/shard_map/all_gather | solution.py:86
  407.0 12.5 %fusion.29 = f32[512,2816]{1,0:T(8,128)} fusion(bf16[512,2048]{1,0:T(8,128)(2,1)} %all-gather.10.cloned.1.call-done, bf16[2048,2816]{1,0:T(8,128)(2,1)} %all-gather.12.cloned.1.call-done), kind=kOutput, calls=%fused_computation.48 | convolution fusion | flops 5905580032 | bytes 19398656 | tf_op jit(solution)/shard_map/dot_general | solution.py:84
  419.5 80.7 %all-gather.14.cloned.1.call-done = bf16[1408,2048]{1,0:T(8,128)(2,1)} async-done(((bf16[1408,256]{1,0:T(8,128)(2,1)}), bf16[1408,2048]{1,0:T(8,128)(2,1)}) %all-gather.14.cloned.1.call-update) | async-done | bytes 5767184 | tf_op jit(solution)/shard_map/all_gather | solution.py:92
  500.2 9.1 %convolution_convert_fusion.1 = bf16[512,2048]{1,0:T(8,128)(2,1)} fusion(bf16[1408,2048]{1,0:T(8,128)(2,1)} %all-gather.14.cloned.1.call-done, f32[512,2816]{1,0:T(8,128)} %fusion.29), kind=kOutput, calls=%fused_computation.23 | convolution fusion | flops 2958163968 | bytes 13631488 | tf_op jit(solution)/shard_map/dot_general | solution.py:94
  509.4 29.5 %reduce-scatter.5.cloned.1.call-done = bf16[128,2048]{1,0:T(8,128)(2,1)} async-done(((bf16[512,2048]{1,0:T(8,128)(2,1)}), bf16[128,2048]{1,0:T(8,128)(2,1)}) %reduce-scatter.5.cloned.1.call-update) | async-done | bytes 524304 | tf_op jit(solution)/shard_map/reduce_scatter | solution.py:93
  538.9 2.0 fusion.23
  (61 shorter events, 0.5 us)
Async XLA Ops:
  6.5 54.8 %all-gather.6.cloned.1.call-start = ((), (), s32[]{:S(2)}) async-start(), calls=%async_computation.2 | async-start | bytes 2359296 | tf_op jit(solution)/shard_map/all_gather | solution.py:42
  7.3 103.8 %all-gather.8.cloned.1.call-start = ((), (), s32[]{:S(2)}) async-start(), calls=%async_computation.3 | async-start | bytes 2359296 | tf_op jit(solution)/shard_map/all_gather | solution.py:43
  8.0 208.4 %reduce-scatter.3.cloned.1.call-start = ((), (), s32[]{:S(2)}) async-start(), calls=%async_computation.4 | async-start | bytes 2621440 | tf_op jit(solution)/shard_map/reduce_scatter | solution.py:69
  117.7 4.2 copy-start
  126.1 4.2 copy-start
  134.5 4.2 copy-start
  142.9 4.2 copy-start
  151.3 4.2 copy-start
  159.7 4.2 copy-start
  168.1 4.2 copy-start
  176.5 4.2 copy-start
  182.2 0.7 copy-start.4
  182.2 0.8 copy-start.5
  186.5 31.4 %copy-start.3 = (f32[2048]{0:T(1024)S(1)}, f32[2048]{0:T(1024)}, u32[]{:S(2)}) copy-start(f32[2048]{0:T(1024)} %param.20) | copy-start | bytes 24580
  186.5 32.4 %copy-start.1 = (bf16[256,1408]{1,0:T(8,128)(2,1)S(1)}, bf16[256,1408]{1,0:T(8,128)(2,1)}, u32[]{:S(2)}) copy-start(bf16[256,1408]{1,0:T(8,128)(2,1)} %param.22) | copy-start | bytes 2162692
  186.5 32.4 %copy-start.2 = (bf16[256,1408]{1,0:T(8,128)(2,1)S(1)}, bf16[256,1408]{1,0:T(8,128)(2,1)}, u32[]{:S(2)}) copy-start(bf16[256,1408]{1,0:T(8,128)(2,1)} %param.21) | copy-start | bytes 2162692
  186.6 55.1 %all-gather.10.cloned.1.call-start = ((), (), s32[]{:S(2)}) async-start(), calls=%async_computation.5 | async-start | bytes 2621440 | tf_op jit(solution)/shard_map/all_gather | solution.py:79
  218.9 188.1 %all-gather.12.cloned.1.call-start = ((), (), s32[]{:S(2)}) async-start(), calls=%async_computation.6 | async-start | bytes 12976128 | tf_op jit(solution)/shard_map/all_gather | solution.py:86
  220.2 280.0 %all-gather.14.cloned.1.call-start = ((), (), s32[]{:S(2)}) async-start(), calls=%async_computation.7 | async-start | bytes 6488064 | tf_op jit(solution)/shard_map/all_gather | solution.py:92
  220.8 318.1 %reduce-scatter.5.cloned.1.call-start = ((), (), s32[]{:S(2)}) async-start(), calls=%async_computation.8 | async-start | bytes 2621440 | tf_op jit(solution)/shard_map/reduce_scatter | solution.py:93
Sparse Core Ops, SparseCore 0:
  9.5 51.7 all-gather.5
  63.4 47.6 all-gather.7
  186.7 29.6 reduce-scatter.2
  219.0 22.5 all-gather.9
  243.7 163.2 all-gather.11
  408.9 91.2 all-gather.13
  509.5 29.3 reduce-scatter.4
where the time goes:
time: 548 us
  waiting for transfers between devices  412 us (75%)
  matrix products  57.9 us (11%)
  local copies, waits for them, and re-layouts  32.1 us (6%)
  other arithmetic  30.8 us (6%)
  between operations  13.6 us (2%)
    all_gather x1, waiting for transfers between devices, per_device(): lax.all_gather(joined, 'sp', axis=0, tiled=True)  165 us
    all_gather x1, waiting for transfers between devices, per_device(): down_whole = lax.all_gather(w_down, 'sp', axis=1, tiled=True)  80.7 us
    all_gather x1, waiting for transfers between devices, per_device(): key_piece = lax.all_gather(key_pairs, 'sp', axis=0, tiled=True)  52.1 us
    all_gather x1, waiting for transfers between devices, per_device(): value_piece = lax.all_gather(values, 'sp', axis=0, tiled=True)  32.4 us
    reduce_scatter x1, waiting for transfers between devices, per_device(): lax.psum_scatter(jnp.dot(heads_out, w_mine, preferred_element_type=jnp.fl...  29.8 us
    reduce_scatter x1, waiting for transfers between devices, per_device(): lax.psum_scatter(jnp.dot(hidden_units, down_whole, preferred_element_type...  29.5 us
    reduce_sum x8, other arithmetic, update(): totals = totals * shrink + jnp.sum(weights, axis=-1)  24.3 us
    dot_general x8, matrix products, update(): jnp.einsum('qhmd,khmd->hmqk', query_view, key_block, preferred_element_ty...  21.7 us
  transfers between devices with their start and end apart: 7, of which 7 were waited for; matrix products, arithmetic and copies ran while one was open for 6% of the time, Pallas kernels for 0%

commit v1 on v0

--- a/solution.py
+++ b/solution.py
@@ -89,7 +89,7 @@
     gate_sum = both_sums[:, :unit_width]
     up_sum = both_sums[:, unit_width:]
     hidden_units = (jax.nn.silu(gate_sum) * up_sum).astype(jnp.bfloat16)
-    down_whole = lax.all_gather(w_down, "sp", axis=1, tiled=True)
+    down_whole = jnp.concatenate(lax.all_gather(w_down, "sp"), axis=1)
     ffn_out = lax.psum_scatter(
         jnp.dot(hidden_units, down_whole, preferred_element_type=jnp.float32).astype(jnp.bfloat16),
         "tp",

time: 548 us -> 553 us (level)
  local copies, waits for them, and re-layouts: 32.1 us -> 40.4 us
  matrix products: 57.9 us -> 51.2 us
    all_gather x1, waiting for transfers between devices: 80.7 us -> 90.5 us  [per_device(): down_whole = jnp.concatenate(lax.all_gather(w_down, 'sp'), axis=1)]
    reshape x0 -> x1, local copies, waits for them, and re-layouts: none -> 8.27 us  [per_device(): down_whole = jnp.concatenate(lax.all_gather(w_down, 'sp'), axis=1)]
    all_gather x1, waiting for transfers between devices: 20.6 us -> 13.9 us  [per_device(): lax.all_gather((scaled * norm_gain).astype(jnp.bfloat16), 'tp', axis=0, t...]
where the time goes in v1:
time: 553 us; the launch traced here: 552 us
  waiting for transfers between devices  415 us (75%)
  matrix products  51.2 us (9%)
  local copies, waits for them, and re-layouts  40.4 us (7%)
  other arithmetic  30.8 us (6%)
  between operations  13.6 us (2%)
    all_gather x1, waiting for transfers between devices, per_device(): lax.all_gather(joined, 'sp', axis=0, tiled=True)  165 us
    all_gather x1, waiting for transfers between devices, per_device(): down_whole = jnp.concatenate(lax.all_gather(w_down, 'sp'), axis=1)  90.5 us
    all_gather x1, waiting for transfers between devices, per_device(): key_piece = lax.all_gather(key_pairs, 'sp', axis=0, tiled=True)  52.1 us
    all_gather x1, waiting for transfers between devices, per_device(): value_piece = lax.all_gather(values, 'sp', axis=0, tiled=True)  32.4 us
    reduce_scatter x1, waiting for transfers between devices, per_device(): lax.psum_scatter(jnp.dot(hidden_units, down_whole, preferred_element_type...  29.5 us
    reduce_scatter x1, waiting for transfers between devices, per_device(): lax.psum_scatter(jnp.dot(heads_out, w_mine, preferred_element_type=jnp.fl...  29.2 us
    reduce_sum x8, other arithmetic, update(): totals = totals * shrink + jnp.sum(weights, axis=-1)  24.3 us
    dot_general x8, matrix products, update(): jnp.einsum('qhmd,khmd->hmqk', query_view, key_block, preferred_element_ty...  21.7 us
  transfers between devices with their start and end apart: 7, of which 7 were waited for; matrix products, arithmetic and copies ran while one was open for 6% of the time, Pallas kernels for 0%

profile of v1, /device:TPU:0, one launch (start us, length us, event | category | flops | bytes accessed | tf_op | source)
XLA Modules:
  0.0 551.6 jit_solution(15107782710235911323)
XLA Ops:
  6.5 0.7 all-gather.7.cloned.1.call-update
  7.3 0.7 all-gather.9.cloned.1.call-update
  8.0 0.0 reduce-scatter.3.cloned.1.call-start
  8.1 1.1 copy.25
  9.2 52.1 %all-gather.7.cloned.1.call-done = bf16[4096,256]{1,0:T(8,128)(2,1)} async-done(((bf16[512,256]{1,0:T(8,128)(2,1)}), bf16[4096,256]{1,0:T(8,128)(2,1)}) %all-gather.7.cloned.1.call-update) | async-done | bytes 2097168 | tf_op jit(solution)/shard_map/all_gather | solution.py:42
  61.3 8.3 %reshape.46 = bf16[8,512,2,2,64]{4,3,2,1,0:T(2,128)(2,1)} reshape(bf16[4096,256]{1,0:T(8,128)(2,1)} %all-gather.7.cloned.1.call-done) | data formatting | bytes 4194304 | tf_op jit(solution)/shard_map/reshape | solution.py:46
  69.6 9.1 %copy.27 = bf16[8,512,2,2,64]{1,4,3,2,0:T(8,128)(2,1)S(1)} copy(bf16[8,512,2,2,64]{4,3,2,1,0:T(2,128)(2,1)} %reshape.46) | data formatting | bytes 4194304
  78.7 32.4 %all-gather.9.cloned.1.call-done = bf16[4096,256]{1,0:T(8,128)(2,1)} async-done(((bf16[512,256]{1,0:T(8,128)(2,1)}), bf16[4096,256]{1,0:T(8,128)(2,1)}) %all-gather.9.cloned.1.call-update) | async-done | bytes 2097168 | tf_op jit(solution)/shard_map/all_gather | solution.py:43
  111.1 4.0 reshape.47
  115.1 67.1 %while.18 = (s32[]{:T(128)}, f32[2,2,512]{2,1,0:T(2,128)S(1)}, f32[2,2,512]{2,1,0:T(2,128)S(1)}, f32[2,2,512,128]{3,2,1,0:T(8,128)S(1)}, bf16[8,512,2,2,64]{1,4,...) while((s32[]{:T(128)}, f32[2,2,512]{2,1,0:T(2,128)S(1)}, ...), condition=%wide.region_3.0_spmd.clone, body=%wide.region_0.0_spmd.clone.sunk | while | flops 411838464 | bytes 32899212 | solution.py:52
  115.1 2.7 bitcast_reduce_fusion.2
  117.8 3.0 fusion.44
  120.9 1.1 constant_dynamic-slice_fusion.2
  122.0 1.4 fusion.46
  123.4 2.7 bitcast_reduce_fusion.2
  126.2 3.0 fusion.44
  129.2 1.1 constant_dynamic-slice_fusion.2
  130.4 1.4 fusion.46
  131.8 2.7 bitcast_reduce_fusion.2
  134.6 3.0 fusion.44
  137.6 1.1 constant_dynamic-slice_fusion.2
  138.8 1.4 fusion.46
  140.2 2.7 bitcast_reduce_fusion.2
  143.0 3.0 fusion.44
  146.0 1.1 constant_dynamic-slice_fusion.2
  147.2 1.4 fusion.46
  148.6 2.7 bitcast_reduce_fusion.2
  151.3 3.0 fusion.44
  154.4 1.1 constant_dynamic-slice_fusion.2
  155.6 1.4 fusion.46
  157.0 2.7 bitcast_reduce_fusion.2
  159.7 3.0 fusion.44
  162.8 1.1 constant_dynamic-slice_fusion.2
  164.0 1.4 fusion.46
  165.4 2.7 bitcast_reduce_fusion.2
  168.1 3.0 fusion.44
  171.2 1.1 constant_dynamic-slice_fusion.2
  172.4 1.4 fusion.46
  173.8 2.7 bitcast_reduce_fusion.2
  176.5 3.0 fusion.44
  179.6 1.1 constant_dynamic-slice_fusion.2
  180.7 1.4 fusion.46
  182.2 0.3 copy.30
  182.6 0.2 broadcast_divide_fusion
  182.7 0.1 copy-done.5
  182.8 0.2 multiply_reduce_fusion
  183.0 0.1 multiply_convert_fusion
  183.2 3.3 convolution_convert_fusion
  186.5 0.0 all-gather.15.cloned.1.call-start
  186.6 0.5 all-gather.15.cloned.1.call-update
  187.2 29.2 %reduce-scatter.3.cloned.1.call-done = bf16[128,2048]{1,0:T(8,128)(2,1)} async-done(((bf16[512,2048]{1,0:T(8,128)(2,1)}), bf16[128,2048]{1,0:T(8,128)(2,1)}) %reduce-scatter.3.cloned.1.call-update) | async-done | bytes 524304 | tf_op jit(solution)/shard_map/reduce_scatter | solution.py:69
  216.4 1.5 fusion.20
  217.9 1.0 fusion.22
  218.9 0.0 all-gather.13.cloned.1.call-start
  219.0 1.3 pad_maximum_fusion
  220.3 0.0 reduce-scatter.5.cloned.1.call-start
  220.3 90.5 %all-gather.15.cloned.1.call-done = bf16[11264,256]{1,0:T(8,128)(2,1)} async-done(((bf16[1408,256]{1,0:T(8,128)(2,1)}), bf16[11264,256]{1,0:T(8,128)(2,1)}) %all-gather.15.cloned.1.call-update) | async-done | bytes 5767184 | tf_op jit(solution)/shard_map/all_gather | solution.py:92
  310.8 8.3 %copy.31 = bf16[1408,8,256]{0,2,1:T(8,128)(2,1)} copy(bf16[1408,8,256]{2,0,1:T(8,128)(2,1)} %bitcast.67) | data formatting | bytes 11534336 | tf_op jit(solution)/shard_map/reshape | solution.py:92
  319.0 13.9 %all-gather.11.cloned.1.call-done = bf16[512,2048]{1,0:T(8,128)(2,1)} async-done(((bf16[128,2048]{1,0:T(8,128)(2,1)}), bf16[512,2048]{1,0:T(8,128)(2,1)}) %all-gather.11.cloned.1.call-update) | async-done | bytes 2097168 | tf_op jit(solution)/shard_map/all_gather | solution.py:79
  333.0 165.4 %all-gather.13.cloned.1.call-done = bf16[2048,2816]{1,0:T(8,128)(2,1)} async-done(((bf16[256,2816]{1,0:T(8,128)(2,1)}), bf16[2048,2816]{1,0:T(8,128)(2,1)}) %all-gather.13.cloned.1.call-update) | async-done | bytes 11534352 | tf_op jit(solution)/shard_map/all_gather | solution.py:86
  498.3 10.3 %fusion.29 = f32[512,2816]{1,0:T(8,128)S(1)} fusion(bf16[512,2048]{1,0:T(8,128)(2,1)} %all-gather.11.cloned.1.call-done, bf16[2048,2816]{1,0:T(8,128)(2,1)} %all-gather.13.cloned.1.call-done), kind=kOutput, calls=%fused_computation.48 | convolution fusion | flops 5905580032 | bytes 19398656 | tf_op jit(solution)/shard_map/dot_general | solution.py:84
  508.6 4.7 convolution_convert_fusion.1
  513.4 29.5 %reduce-scatter.5.cloned.1.call-done = bf16[128,2048]{1,0:T(8,128)(2,1)} async-done(((bf16[512,2048]{1,0:T(8,128)(2,1)}), bf16[128,2048]{1,0:T(8,128)(2,1)}) %reduce-scatter.5.cloned.1.call-update) | async-done | bytes 524304 | tf_op jit(solution)/shard_map/reduce_scatter | solution.py:93
  542.8 2.0 fusion.23
  (64 shorter events, 0.5 us)
Async XLA Ops:
  6.5 54.8 %all-gather.7.cloned.1.call-start = ((), (), s32[]{:S(2)}) async-start(), calls=%async_computation.2 | async-start | bytes 2359296 | tf_op jit(solution)/shard_map/all_gather | solution.py:42
  7.3 103.8 %all-gather.9.cloned.1.call-start = ((), (), s32[]{:S(2)}) async-start(), calls=%async_computation.3 | async-start | bytes 2359296 | tf_op jit(solution)/shard_map/all_gather | solution.py:43
  8.0 208.4 %reduce-scatter.3.cloned.1.call-start = ((), (), s32[]{:S(2)}) async-start(), calls=%async_computation.4 | async-start | bytes 2621440 | tf_op jit(solution)/shard_map/reduce_scatter | solution.py:69
  117.8 4.2 copy-start
  126.2 4.2 copy-start
  134.5 4.2 copy-start
  142.9 4.2 copy-start
  151.3 4.2 copy-start
  159.7 4.2 copy-start
  168.1 4.2 copy-start
  176.5 4.2 copy-start
  182.2 0.7 copy-start.5
  182.2 0.8 copy-start.6
  186.5 31.4 %copy-start.4 = (f32[2048]{0:T(1024)S(1)}, f32[2048]{0:T(1024)}, u32[]{:S(2)}) copy-start(f32[2048]{0:T(1024)} %param.20) | copy-start | bytes 24580
  186.5 32.4 %copy-start.2 = (bf16[256,1408]{1,0:T(8,128)(2,1)S(1)}, bf16[256,1408]{1,0:T(8,128)(2,1)}, u32[]{:S(2)}) copy-start(bf16[256,1408]{1,0:T(8,128)(2,1)} %param.22) | copy-start | bytes 2162692
  186.5 32.4 %copy-start.3 = (bf16[256,1408]{1,0:T(8,128)(2,1)S(1)}, bf16[256,1408]{1,0:T(8,128)(2,1)}, u32[]{:S(2)}) copy-start(bf16[256,1408]{1,0:T(8,128)(2,1)} %param.21) | copy-start | bytes 2162692
  186.5 124.2 %all-gather.15.cloned.1.call-start = ((), (), s32[]{:S(2)}) async-start(), calls=%async_computation.8 | async-start | bytes 6488064 | tf_op jit(solution)/shard_map/all_gather | solution.py:92
  187.1 145.8 %all-gather.11.cloned.1.call-start = ((), (), s32[]{:S(2)}) async-start(), calls=%async_computation.5 | async-start | bytes 2621440 | tf_op jit(solution)/shard_map/all_gather | solution.py:79
  218.9 279.5 %all-gather.13.cloned.1.call-start = ((), (), s32[]{:S(2)}) async-start(), calls=%async_computation.6 | async-start | bytes 12976128 | tf_op jit(solution)/shard_map/all_gather | solution.py:86
  220.3 322.6 %reduce-scatter.5.cloned.1.call-start = ((), (), s32[]{:S(2)}) async-start(), calls=%async_computation.7 | async-start | bytes 2621440 | tf_op jit(solution)/shard_map/reduce_scatter | solution.py:93
  498.3 10.3 %copy-start.1 = (bf16[1408,8,256]{0,2,1:T(8,128)(2,1)S(1)}, bf16[1408,8,256]{0,2,1:T(8,128)(2,1)}, u32[]{:S(2)}) copy-start(bf16[1408,8,256]{0,2,1:T(8,128)(2,1)} %copy.31) | copy-start | bytes 17301508
Sparse Core Ops, SparseCore 0:
  9.5 51.7 all-gather.6
  63.4 47.6 all-gather.8
  186.7 29.6 reduce-scatter.2
  218.4 92.2 all-gather.14
  312.2 20.7 all-gather.10
  335.0 163.2 all-gather.12
  513.5 29.3 reduce-scatter.4
